TPU v7x, 32 devices: a whole 2x2x4 slice. The times are simulated.
32 devices in a mesh: sp: 4 (over x, core), dp: 8 (over z, y).
Axes of the slice: x: 2, y: 2, z: 4, core: 2. Of those that a mesh axis runs over, the one named last changes fastest.
Arguments:
- query: bfloat16 [8, 512, 1024], P('dp', None, 'sp'), may hold values from -120 to 120
- keys: bfloat16 [8, 512, 1024], P('dp', None, 'sp'), may hold values from -6 to 6
- values: bfloat16 [8, 512, 1024], P('dp', None, 'sp'), may hold values from -6 to 6
- output: bfloat16 [8, 512, 1024], P('dp'), may hold values from -1 to 1
- cum: float32 [8, 16, 512], P('dp', 'sp'), as said below
- d_out: bfloat16 [8, 512, 2048], P('dp', 'sp'), may hold values from -6 to 6
- w_out: bfloat16 [1024, 2048], P('dp'), may hold values from -0.125 to 0.125
Outputs:
- d_query: bfloat16 [8, 512, 1024], P('dp', 'sp')
- d_key: bfloat16 [8, 512, 1024], P('dp', 'sp')
- d_value: bfloat16 [8, 512, 1024], P('dp', 'sp')
- d_cum: float32 [8, 16, 512], P('dp', 'sp')
- d_w_out: float32 [1024, 2048], P('dp', 'sp')
Inputs may be any that keep to these rules, and one draw needn't show every extreme that they name: cum never rises along positions.
All inputs are finite; a program needn't handle non-finite values.
Results may differ from a plain program's by a relative error of at most 0.008.
Values may be sent and summed in bfloat16 or wider, within the bound.
A program may use at most 64 MiB of HBM per device.

v0:
```python
import jax
import jax.numpy as jnp
from jax import lax
from jax.sharding import PartitionSpec as P


def head_grads(query, keys, values, output, cotangent, cum):
    head_count, length, head_width = query.shape
    span_rows = min(512, length)
    score_scale = head_width ** (-0.5)
    row_dots = jnp.sum(cotangent.astype(jnp.float32) * output.astype(jnp.float32), axis=2)
    positions = jnp.arange(length)

    def product(left, right, form):
        return jnp.einsum(form, left, right, preferred_element_type=jnp.float32)

    def advance(totals, block_index):
        key_grad, value_grad, cum_grad = totals
        offset = block_index * span_rows
        query_blk = lax.dynamic_slice_in_dim(query, offset, span_rows, 1)
        cot_blk = lax.dynamic_slice_in_dim(cotangent, offset, span_rows, 1)
        cum_blk = lax.dynamic_slice_in_dim(cum, offset, span_rows, 1)
        dots_blk = lax.dynamic_slice_in_dim(row_dots, offset, span_rows, 1)
        scores = product(query_blk, keys, "hqe,hke->hqk") * score_scale
        scores = scores + cum_blk[:, :, None] - cum[:, None, :]
        query_pos = offset + jnp.arange(span_rows)
        causal = positions[None, :] <= query_pos[:, None]
        scores = jnp.where(causal[None], scores, -1e30)
        row_max = jnp.max(scores, axis=2, keepdims=True)
        weights = jnp.exp(scores - row_max)
        weights = weights / jnp.sum(weights, axis=2, keepdims=True)
        weights_b = weights.astype(jnp.bfloat16)
        d_prob = product(cot_blk, values, "hqe,hke->hqk")
        d_score = weights * (d_prob - dots_blk[:, :, None])
        score_b = d_score.astype(jnp.bfloat16)
        query_grad = (product(score_b, keys, "hqk,hke->hqe") * score_scale).astype(jnp.bfloat16)
        key_grad = key_grad + product(score_b, query_blk, "hqk,hqe->hke") * score_scale
        value_grad = value_grad + product(weights_b, cot_blk, "hqk,hqe->hke")
        cum_grad = cum_grad - jnp.sum(d_score, axis=1)
        own_part = lax.dynamic_slice_in_dim(cum_grad, offset, span_rows, 1) + jnp.sum(
            d_score, axis=2
        )
        cum_grad = lax.dynamic_update_slice_in_dim(cum_grad, own_part, offset, 1)
        return ((key_grad, value_grad, cum_grad), query_grad)

    start_state = (
        jnp.zeros(query.shape, jnp.float32),
        jnp.zeros(query.shape, jnp.float32),
        jnp.zeros(cum.shape, jnp.float32),
    )
    totals, query_blocks = lax.scan(advance, start_state, jnp.arange(length // span_rows))
    query_grad = jnp.transpose(query_blocks, (1, 0, 2, 3)).reshape(query.shape)
    return (query_grad, totals[0].astype(jnp.bfloat16), totals[1].astype(jnp.bfloat16), totals[2])


def shards(query, keys, values, output, cum, d_out, w_out):
    local_rows = d_out[0]
    whole_output = output[0]
    d_attn = lax.dot_general(
        local_rows,
        lax.all_gather(w_out, "dp", axis=0, tiled=True),
        (((1,), (1,)), ((), ())),
        preferred_element_type=jnp.float32,
    ).astype(jnp.bfloat16)
    head_cot, column_part = (
        lax.all_to_all(d_attn[None], "sp", split_axis=2, concat_axis=1, tiled=True),
        lax.all_to_all(d_out, "sp", split_axis=2, concat_axis=1, tiled=True),
    )
    grad_weight = lax.psum_scatter(
        lax.dot_general(
            whole_output,
            column_part[0],
            (((0,), (0,)), ((), ())),
            preferred_element_type=jnp.float32,
        ),
        "dp",
        scatter_dimension=0,
        tiled=True,
    )
    head_cols = query.shape[2]
    head_count = cum.shape[1]
    head_width = head_cols // head_count
    seq_length = query.shape[1]
    own_output = lax.dynamic_slice_in_dim(
        whole_output, lax.axis_index("sp") * head_cols, head_cols, 1
    )

    def heads_first(matrix):
        return jnp.transpose(matrix.reshape(seq_length, head_count, head_width), (1, 0, 2))

    def tokens_first(matrix):
        return jnp.transpose(matrix, (1, 0, 2)).reshape(1, seq_length, head_cols)

    grads = head_grads(
        heads_first(query[0]),
        heads_first(keys[0]),
        heads_first(values[0]),
        heads_first(own_output),
        heads_first(head_cot[0]),
        cum[0],
    )
    query_grad, key_grad, value_grad = (
        lax.all_to_all(tokens_first(grads[0]), "sp", split_axis=1, concat_axis=2, tiled=True),
        lax.all_to_all(tokens_first(grads[1]), "sp", split_axis=1, concat_axis=2, tiled=True),
        lax.all_to_all(tokens_first(grads[2]), "sp", split_axis=1, concat_axis=2, tiled=True),
    )
    return (query_grad, key_grad, value_grad, grads[3][None], grad_weight)


def solution(mesh):
    placed = (
        P("dp", None, "sp"),
        P("dp", None, "sp"),
        P("dp", None, "sp"),
        P("dp", None, None),
        P("dp", "sp", None),
        P("dp", "sp", None),
        P("dp", None),
    )
    return jax.shard_map(
        shards,
        mesh=mesh,
        in_specs=placed,
        out_specs=(
            P("dp", "sp", None),
            P("dp", "sp", None),
            P("dp", "sp", None),
            P("dp", "sp", None),
            P("dp", "sp"),
        ),
        check_vma=False,
    )
```

profile of v0, /device:TPU:0, one launch (start us, length us, event | category | flops | bytes accessed | tf_op | source)
XLA Modules:
  0.0 163.5 jit_solution(12182984740562545491)
XLA Ops:
  7.2 0.0 all-gather.2.cloned.1.call-start
  7.2 0.7 all-gather.2.cloned.1.call-update
  7.9 0.0 reduce-scatter.2.cloned.1.call-start
  7.9 2.4 %copy.99 = bf16[1,128,2048]{1,0,2:T(2,128)(2,1)S(1)} copy(bf16[1,128,2048]{2,1,0:T(8,128)(2,1)} %param.12) | data formatting | bytes 1048576 | tf_op args[5]
  10.3 0.0 copy-start.1
  10.3 0.5 broadcast.48
  10.8 11.5 %reduce.4 = bf16[2048,128]{1,0:T(8,128)(2,1)S(1)} reduce(bf16[2048,1,128]{2,1,0:T(2,128)(2,1)S(1)} %bitcast.83, bf16[]{:T(256)} %broadcast.48), dimensions={1}, to_apply=%bitcast.67.reduce_sub_computation | reduce | bytes 1048578
  22.4 0.1 reshape.79
  22.5 12.9 %all_to_all.84 = bf16[4,2,32768]{2,1,0:T(2,128)(2,1)S(1)} all-to-all(bf16[4,2,32768]{2,1,0:T(2,128)(2,1)S(1)} %reshape.79), channel_id=1, replica_groups=mesh['sp'=4,'dp'=8] {'sp'}, dimensions={0} | all-to-all | bytes 1048576 | tf_op jit(solution)/shard_map/all_to_all | solution.py:67
  35.3 0.5 reshape.80
  35.9 0.1 copy.112
  35.9 0.0 copy-start.4
  36.0 0.2 copy.100
  36.2 0.0 copy-start
  36.2 2.1 %fusion.15 = f32[1024,512]{1,0:T(8,128)} fusion(bf16[512,512]{1,0:T(8,128)(2,1)S(1)} %bitcast.85, bf16[1,512,1024]{2,1,0:T(8,128)(2,1)S(1)} %copy-done.1), kind=kOutput, calls=%fused_computation.20 | convolution fusion | flops 536870912 | bytes 3670016 | tf_op jit(solution)/shard_map/dot_general | solution.py:70
  38.3 0.0 reduce-scatter.2.cloned.1.call-update
  38.4 0.2 copy.88
  38.6 0.1 copy.83
  38.8 0.1 copy.84
  38.9 0.0 copy-start.8
  38.9 0.8 copy.87
  39.8 0.1 iota_compare_fusion
  39.9 45.8 %all-gather.2.cloned.1.call-done = bf16[1024,2048]{1,0:T(8,128)(2,1)} async-done(((bf16[128,2048]{1,0:T(8,128)(2,1)}), bf16[1024,2048]{1,0:T(8,128)(2,1)}) %all-gather.2.cloned.1.call-update) | async-done | bytes 4194320 | tf_op jit(solution)/shard_map/all_gather | solution.py:61
  85.7 3.7 %fusion.14 = bf16[1,128,1024]{2,1,0:T(8,128)(2,1)S(1)} fusion(bf16[1024,2048]{1,0:T(8,128)(2,1)} %all-gather.2.cloned.1.call-done, bf16[1,128,2048]{2,1,0:T(8,128)(2,1)S(1)} %copy-done), kind=kOutput, calls=%fused_computation.19 | convolution fusion | flops 537001984 | bytes 4980736 | tf_op jit(solution)/shard_map/dot_general | solution.py:59
  89.4 0.4 copy.85
  89.8 2.2 %reduce = bf16[1024,128]{1,0:T(8,128)(2,1)S(1)} reduce(bf16[1024,1,128]{2,1,0:T(2,128)(2,1)S(1)} %bitcast.92, bf16[]{:T(256)} %broadcast.48), dimensions={1}, to_apply=%bitcast.59.reduce_sub_computation | reduce | bytes 524290
  92.0 0.8 reshape.71
  92.8 3.6 %all-to-all-start = ((bf16[4,2,16384]{2,1,0:T(2,128)(2,1)}), bf16[4,2,16384]{2,1,0:T(2,128)(2,1)S(1)}, u32[]{:S(2)}, u32[]{:S(2)}) async-start(bf16[4,2,16384]{2,1,0:T(2,128)(2,1)} %reshape.71), calls=%async_computation | async-start | bytes 524288 | tf_op jit(solution)/shard_map/all_to_all | solution.py:66
  96.4 3.4 %fusion.32 = (f32[4,512]{1,0:T(4,128)S(1)}, f32[4,512,512]{1,2,0:T(8,128)}) fusion(f32[4,512]{1,0:T(4,128)S(1)} %bitcast.112, pred[512,512]{0,1:T(8,128)(4,1)S(1)} %iota_compare_fusion, bf16[4,512,64]{1,2,0:T(8,128)(2,1)S(1)} %bitcast.97, bf16[4,512,64]{1,2,0:T(8,128)(2,1)S(1)} %bitcast.100), kind=kOutput, calls=%fused_computation.38 | convolution fusion | flops 140509696 | bytes 4997120 | tf_op jit(solution)/shard_map/while/body/eval_jaxpr/sub | solution.py:30
  99.8 2.3 %all-to-all-done = bf16[4,2,16384]{2,1,0:T(2,128)(2,1)S(1)} async-done(((bf16[4,2,16384]{2,1,0:T(2,128)(2,1)}), bf16[4,2,16384]{2,1,0:T(2,128)(2,1)S(1)}, u32[]{:S(2)}, u32[]{:S(2)}) %all-to-all-start) | async-done | bytes 262176 | tf_op jit(solution)/shard_map/all_to_all | solution.py:66
  102.2 0.3 reshape.72
  102.5 0.2 copy.86
  102.7 0.1 reshape_squeeze.14
  102.8 0.0 copy-start.2
  102.8 0.1 multiply_reduce_fusion
  102.9 3.5 %fusion.31 = (f32[4,512]{1,0:T(4,128)S(1)}, f32[4,512]{1,0:T(4,128)S(1)}, bf16[4,512,512]{1,2,0:T(8,128)(2,1)S(1)}) fusion(f32[4,512]{1,0:T(4,128)S(1)} %multiply_reduce_fusion, bf16[4,512,64]{1,2,0:T(8,128)(2,1)} %bitcast.111, bf16[512,4,64]{0,2,1:T(8,128)(2,1)S(1)} %reshape_squeeze.14, f32[4,512,512]{1,2,0:T(8,128)} %get-tuple-element.52, ...), kind=kOutput, calls=%fused_computation.37 | convolution fusion | flops 140505088 | bytes 6848512 | tf_op jit(solution)/shard_map/while/body/eval_jaxpr/hqe,hke->hqk/dot_general | solution.py:15
  106.4 0.8 fusion.9
  107.2 0.4 copy.94
  107.6 3.0 %reduce.2 = bf16[512,256]{1,0:T(8,128)(2,1)} reduce(bf16[512,1,256]{2,1,0:T(2,128)(2,1)S(1)} %bitcast.93, bf16[]{:T(256)} %broadcast.48), dimensions={1}, to_apply=%bitcast.63.reduce_sub_computation | reduce | bytes 524290
  110.6 1.7 %reshape.75 = bf16[4,2,16384]{2,1,0:T(2,128)(2,1)} reshape(bf16[512,256]{1,0:T(8,128)(2,1)} %reduce.2) | data formatting | bytes 524288
  112.3 3.4 %all-to-all-start.2 = ((bf16[4,2,16384]{2,1,0:T(2,128)(2,1)}), bf16[4,2,16384]{2,1,0:T(2,128)(2,1)S(1)}, u32[]{:S(2)}, u32[]{:S(2)}) async-start(bf16[4,2,16384]{2,1,0:T(2,128)(2,1)} %reshape.75), calls=%async_computation.2 | async-start | bytes 524288 | tf_op jit(solution)/shard_map/all_to_all | solution.py:104
  115.7 0.5 fusion.10
  116.2 0.4 copy.91
  116.6 2.2 %reduce.1 = bf16[512,256]{1,0:T(8,128)(2,1)S(1)} reduce(bf16[512,1,256]{2,1,0:T(2,128)(2,1)S(1)} %bitcast.94, bf16[]{:T(256)} %broadcast.48), dimensions={1}, to_apply=%bitcast.61.reduce_sub_computation | reduce | bytes 524290
  118.8 0.8 reshape.73
  119.6 2.1 %all-to-all-done.2 = bf16[4,2,16384]{2,1,0:T(2,128)(2,1)S(1)} async-done(((bf16[4,2,16384]{2,1,0:T(2,128)(2,1)}), bf16[4,2,16384]{2,1,0:T(2,128)(2,1)S(1)}, u32[]{:S(2)}, u32[]{:S(2)}) %all-to-all-start.2) | async-done | bytes 262176 | tf_op jit(solution)/shard_map/all_to_all | solution.py:104
  121.7 3.4 %all-to-all-start.1 = ((bf16[4,2,16384]{2,1,0:T(2,128)(2,1)}), bf16[4,2,16384]{2,1,0:T(2,128)(2,1)S(1)}, u32[]{:S(2)}, u32[]{:S(2)}) async-start(bf16[4,2,16384]{2,1,0:T(2,128)(2,1)} %reshape.73), calls=%async_computation.1 | async-start | bytes 524288 | tf_op jit(solution)/shard_map/all_to_all | solution.py:103
  125.1 3.2 %fusion.11 = bf16[4,512,64]{1,2,0:T(8,128)(2,1)S(1)} fusion(f32[4,512]{1,0:T(4,128)S(1)} %get-tuple-element.38, bf16[512,4,64]{0,2,1:T(8,128)(2,1)S(1)} %copy-done.3, f32[4,512]{1,0:T(4,128)S(1)} %bitcast.113, pred[512,512]{0,1:T(8,128)(4,1)} %copy-done.7, bf16[4,512,64]{1,2,0:T(8,128)(2,1)S(1)} %bitcast.99, bf16[4,512,64]{1,2,0:T(8,128)(2,1)S(1)} %bitcast.102), kind=kOutput, calls=%fused_computation.18 | convolution fusion | flops 275909120 | bytes 1327104 | tf_op jit(solution)/shard_map/while/body/eval_jaxpr/hqk,hqe->hke/dot_general | solution.py:15
  128.3 0.4 copy.97
  128.8 2.2 %reduce.3 = bf16[512,256]{1,0:T(8,128)(2,1)S(1)} reduce(bf16[512,1,256]{2,1,0:T(2,128)(2,1)S(1)} %bitcast.91, bf16[]{:T(256)} %broadcast.48), dimensions={1}, to_apply=%bitcast.65.reduce_sub_computation | reduce | bytes 524290
  131.0 0.8 reshape.77
  131.7 3.4 %all-to-all-start.3 = ((bf16[4,2,16384]{2,1,0:T(2,128)(2,1)}), bf16[4,2,16384]{2,1,0:T(2,128)(2,1)S(1)}, u32[]{:S(2)}, u32[]{:S(2)}) async-start(bf16[4,2,16384]{2,1,0:T(2,128)(2,1)} %reshape.77), calls=%async_computation.3 | async-start | bytes 524288 | tf_op jit(solution)/shard_map/all_to_all | solution.py:105
  135.2 0.6 add_bitcast_fusion
  135.8 0.3 reshape.76
  136.1 0.2 copy.95
  136.3 0.9 copy.102
  137.1 0.3 reshape.74
  137.4 0.2 copy.92
  137.6 0.9 copy.101
  138.5 2.7 %all-to-all-done.3 = bf16[4,2,16384]{2,1,0:T(2,128)(2,1)S(1)} async-done(((bf16[4,2,16384]{2,1,0:T(2,128)(2,1)}), bf16[4,2,16384]{2,1,0:T(2,128)(2,1)S(1)}, u32[]{:S(2)}, u32[]{:S(2)}) %all-to-all-start.3) | async-done | bytes 262176 | tf_op jit(solution)/shard_map/all_to_all | solution.py:105
  141.1 0.3 reshape.78
  141.4 0.2 copy.98
  141.6 0.9 copy.103
  142.5 14.2 %reduce-scatter.2.cloned.1.call-done = f32[128,512]{1,0:T(8,128)} async-done(((f32[1024,512]{1,0:T(8,128)}), f32[128,512]{1,0:T(8,128)}) %reduce-scatter.2.cloned.1.call-update) | async-done | bytes 262160 | tf_op jit(solution)/shard_map/reduce_scatter | solution.py:69
  (19 shorter events, 0.2 us)
Async XLA Ops:
  7.2 78.5 %all-gather.2.cloned.1.call-start = ((), (), s32[]{:S(2)}) async-start(), calls=%async_computation.6 | async-start | bytes 4718592 | tf_op jit(solution)/shard_map/all_gather | solution.py:61
  7.9 148.7 %reduce-scatter.2.cloned.1.call-start = ((), (), s32[]{:S(2)}) async-start(), calls=%async_computation.7 | async-start | bytes 2359296 | tf_op jit(solution)/shard_map/reduce_scatter | solution.py:69
  10.3 25.9 %copy-start.1 = (bf16[1,512,1024]{2,1,0:T(8,128)(2,1)S(1)}, bf16[1,512,1024]{2,1,0:T(8,128)(2,1)}, u32[]{:S(2)}) copy-start(bf16[1,512,1024]{2,1,0:T(8,128)(2,1)} %param.10) | copy-start | bytes 3145732
  35.9 2.6 %copy-start.4 = (bf16[1,512,256]{2,1,0:T(8,128)(2,1)S(1)}, bf16[1,512,256]{2,1,0:T(8,128)(2,1)}, u32[]{:S(2)}) copy-start(bf16[1,512,256]{2,1,0:T(8,128)(2,1)} %param.7) | copy-start | bytes 786436
  36.2 2.6 %copy-start.5 = (bf16[1,512,256]{2,1,0:T(8,128)(2,1)S(1)}, bf16[1,512,256]{2,1,0:T(8,128)(2,1)}, u32[]{:S(2)}) copy-start(bf16[1,512,256]{2,1,0:T(8,128)(2,1)} %param.8) | copy-start | bytes 786436
  36.2 2.7 %copy-start.6 = (bf16[1,512,256]{2,1,0:T(8,128)(2,1)S(1)}, bf16[1,512,256]{2,1,0:T(8,128)(2,1)}, u32[]{:S(2)}) copy-start(bf16[1,512,256]{2,1,0:T(8,128)(2,1)} %param.9) | copy-start | bytes 786436
  36.2 49.5 %copy-start = (bf16[1,128,2048]{2,1,0:T(8,128)(2,1)S(1)}, bf16[1,128,2048]{2,1,0:T(8,128)(2,1)}, u32[]{:S(2)}) copy-start(bf16[1,128,2048]{2,1,0:T(8,128)(2,1)} %param.12) | copy-start | bytes 1572868
  38.9 57.5 %copy-start.8 = (f32[1,4,512]{2,1,0:T(4,128)S(1)}, f32[1,4,512]{2,1,0:T(4,128)}, u32[]{:S(2)}) copy-start(f32[1,4,512]{2,1,0:T(4,128)} %param.11) | copy-start | bytes 24580
  39.9 60.0 %copy-start.7 = (pred[512,512]{0,1:T(8,128)(4,1)}, pred[512,512]{0,1:T(8,128)(4,1)S(1)}, u32[]{:S(2)}) copy-start(pred[512,512]{0,1:T(8,128)(4,1)S(1)} %iota_compare_fusion) | copy-start | bytes 786436
  92.8 9.4 %all-to-all-start = ((bf16[4,2,16384]{2,1,0:T(2,128)(2,1)}), bf16[4,2,16384]{2,1,0:T(2,128)(2,1)S(1)}, u32[]{:S(2)}, u32[]{:S(2)}) async-start(bf16[4,2,16384]{2,1,0:T(2,128)(2,1)} %reshape.71), calls=%async_computation | async-start | bytes 524288 | tf_op jit(solution)/shard_map/all_to_all | solution.py:66
  102.8 3.6 %copy-start.2 = (bf16[512,4,64]{0,2,1:T(8,128)(2,1)}, bf16[512,4,64]{0,2,1:T(8,128)(2,1)S(1)}, u32[]{:S(2)}) copy-start(bf16[512,4,64]{0,2,1:T(8,128)(2,1)S(1)} %reshape_squeeze.14) | copy-start | bytes 786436
  107.6 17.5 %copy-start.3 = (bf16[512,4,64]{0,2,1:T(8,128)(2,1)S(1)}, bf16[512,4,64]{0,2,1:T(8,128)(2,1)}, u32[]{:S(2)}) copy-start(bf16[512,4,64]{0,2,1:T(8,128)(2,1)} %copy-done.2) | copy-start | bytes 786436
  112.3 9.4 %all-to-all-start.2 = ((bf16[4,2,16384]{2,1,0:T(2,128)(2,1)}), bf16[4,2,16384]{2,1,0:T(2,128)(2,1)S(1)}, u32[]{:S(2)}, u32[]{:S(2)}) async-start(bf16[4,2,16384]{2,1,0:T(2,128)(2,1)} %reshape.75), calls=%async_computation.2 | async-start | bytes 524288 | tf_op jit(solution)/shard_map/all_to_all | solution.py:104
  121.7 10.1 %all-to-all-start.1 = ((bf16[4,2,16384]{2,1,0:T(2,128)(2,1)}), bf16[4,2,16384]{2,1,0:T(2,128)(2,1)S(1)}, u32[]{:S(2)}, u32[]{:S(2)}) async-start(bf16[4,2,16384]{2,1,0:T(2,128)(2,1)} %reshape.73), calls=%async_computation.1 | async-start | bytes 524288 | tf_op jit(solution)/shard_map/all_to_all | solution.py:103
  131.7 9.4 %all-to-all-start.3 = ((bf16[4,2,16384]{2,1,0:T(2,128)(2,1)}), bf16[4,2,16384]{2,1,0:T(2,128)(2,1)S(1)}, u32[]{:S(2)}, u32[]{:S(2)}) async-start(bf16[4,2,16384]{2,1,0:T(2,128)(2,1)} %reshape.77), calls=%async_computation.3 | async-start | bytes 524288 | tf_op jit(solution)/shard_map/all_to_all | solution.py:105
Sparse Core Ops, SparseCore 0:
  10.1 75.5 all-gather.1
  89.8 66.8 reduce-scatter.1
where the time goes:
time: 164 us; the launch traced here: 163 us
  waiting for transfers between devices  67.7 us (41%)
  other arithmetic  21.9 us (13%)
  matrix products  17.1 us (10%)
  local copies, waits for them, and re-layouts  15.5 us (9%)
  between operations  14.5 us (9%)
  starting transfers between devices  13.9 us (8%)
  blocking collectives  12.9 us (8%)
    all_gather x1, waiting for transfers between devices, shards(): lax.all_gather(w_out, 'dp', axis=0, tiled=True)  45.8 us
    unnamed x5, other arithmetic  21.1 us
    reduce_scatter x1, waiting for transfers between devices, shards(): lax.psum_scatter(lax.dot_general(whole_output, column_part[0], (((0,), (0...  14.2 us
    all_to_all x1, blocking collectives, shards(): lax.all_to_all(d_out, 'sp', split_axis=2, concat_axis=1, tiled=True)  12.9 us
    unnamed x41, local copies, waits for them, and re-layouts  12.5 us
    dot_general x4, matrix products, product(): return jnp.einsum(form, left, right, preferred_element_type=jnp.float32)  7.92 us
    dot_general x1, matrix products, shards(): lax.dot_general(local_rows, lax.all_gather(w_out, 'dp', axis=0, tiled=Tru...  3.7 us
    all_to_all x1, starting transfers between devices, shards(): lax.all_to_all(d_attn[None], 'sp', split_axis=2, concat_axis=1, tiled=True)  3.6 us
  transfers between devices with their start and end apart: 6, of which 5 were waited for; matrix products, arithmetic and copies ran while one was open for 33% of the time, Pallas kernels for 0%

commit v1 on v0

--- a/solution.py
+++ b/solution.py
@@ -64,7 +64,10 @@
     ).astype(jnp.bfloat16)
     head_cot, column_part = (
         lax.all_to_all(d_attn[None], "sp", split_axis=2, concat_axis=1, tiled=True),
-        lax.all_to_all(d_out, "sp", split_axis=2, concat_axis=1, tiled=True),
+        jnp.concatenate(
+            lax.all_to_all(jnp.stack(jnp.split(d_out, lax.axis_size("sp"), axis=2)), "sp", 0, 0),
+            axis=1,
+        ),
     )
     grad_weight = lax.psum_scatter(
         lax.dot_general(

time: 164 us -> 206 us (1.26)
  waiting for transfers between devices: 67.7 us -> 122 us
  other arithmetic: 21.9 us -> 10.5 us
    reduce_scatter x1, waiting for transfers between devices: 14.2 us -> 56.5 us  [shards(): lax.psum_scatter(lax.dot_general(whole_output, column_part[0], (((0,), (0...]
    all_gather x1, waiting for transfers between devices: 45.8 us -> 59.9 us  [shards(): lax.all_gather(w_out, 'dp', axis=0, tiled=True)]
    unnamed x5 -> x4, other arithmetic: 21.1 us -> 9.59 us
    all_to_all x1, waiting for transfers between devices: 2.34 us -> 0.01 us  [shards(): lax.all_to_all(d_attn[None], 'sp', split_axis=2, concat_axis=1, tiled=True)]
    unnamed x41 -> x38, local copies, waits for them, and re-layouts: 12.5 us -> 11.3 us
  transfers between devices with their start and end apart: 6 -> 6, of which waited for: 5 -> 4; matrix products, arithmetic and copies ran while one was open for 33% -> 15% of each run, Pallas kernels for 0% -> 0%
where the time goes in v1:
time: 206 us
  waiting for transfers between devices  122 us (59%)
  matrix products  17.1 us (8%)
  local copies, waits for them, and re-layouts  15.1 us (7%)
  between operations  14.4 us (7%)
  starting transfers between devices  13.9 us (7%)
  blocking collectives  13 us (6%)
  other arithmetic  10.5 us (5%)
    all_gather x1, waiting for transfers between devices, shards(): lax.all_gather(w_out, 'dp', axis=0, tiled=True)  59.9 us
    reduce_scatter x1, waiting for transfers between devices, shards(): lax.psum_scatter(lax.dot_general(whole_output, column_part[0], (((0,), (0...  56.5 us
    all_to_all x1, blocking collectives, shards(): lax.all_to_all(jnp.stack(jnp.split(d_out, lax.axis_size('sp'), axis=2)),...  13 us
    unnamed x38, local copies, waits for them, and re-layouts  11.3 us
    unnamed x4, other arithmetic  9.59 us
    dot_general x4, matrix products, product(): return jnp.einsum(form, left, right, preferred_element_type=jnp.float32)  7.89 us
  transfers between devices with their start and end apart: 6, of which 4 were waited for; matrix products, arithmetic and copies ran while one was open for 15% of the time, Pallas kernels for 0%

profile of v1, /device:TPU:0, one launch (start us, length us, event | category | flops | bytes accessed | tf_op | source)
XLA Modules:
  0.0 205.6 jit_solution(14533844079328939834)
XLA Ops:
  7.2 0.0 all-gather.2.cloned.1.call-start
  7.2 0.7 all-gather.2.cloned.1.call-update
  7.9 0.0 reduce-scatter.2.cloned.1.call-start
  8.0 1.1 slice_bitcast_fusion.3
  9.1 0.1 pad_maximum_fusion
  9.2 0.0 copy-start.4
  9.2 13.0 %all_to_all.74 = bf16[4,1,128,512]{3,2,1,0:T(8,128)(2,1)S(1)} all-to-all(bf16[4,1,128,512]{3,2,1,0:T(8,128)(2,1)S(1)} %pad_maximum_fusion), channel_id=1, replica_groups=mesh['sp'=4,'dp'=8] {'sp'}, dimensions={0} | all-to-all | bytes 1048576 | tf_op jit(solution)/shard_map/all_to_all | solution.py:68
  22.2 0.0 copy-done.1
  22.2 2.1 convolution_bitcast_fusion
  24.2 0.0 reduce-scatter.2.cloned.1.call-update
  24.3 0.2 copy.74
  24.5 0.1 copy.69
  24.7 0.0 copy-done.5
  24.7 0.1 copy.70
  24.8 0.0 copy-start.8
  24.9 0.8 copy.73
  25.7 0.1 iota_compare_fusion
  25.8 59.9 %all-gather.2.cloned.1.call-done = bf16[1024,2048]{1,0:T(8,128)(2,1)} async-done(((bf16[128,2048]{1,0:T(8,128)(2,1)}), bf16[1024,2048]{1,0:T(8,128)(2,1)}) %all-gather.2.cloned.1.call-update) | async-done | bytes 4194320 | tf_op jit(solution)/shard_map/all_gather | solution.py:61
  85.7 3.7 %fusion.14 = bf16[1,128,1024]{2,1,0:T(8,128)(2,1)S(1)} fusion(bf16[1024,2048]{1,0:T(8,128)(2,1)} %all-gather.2.cloned.1.call-done, bf16[1,128,2048]{2,1,0:T(8,128)(2,1)S(1)} %copy-done), kind=kOutput, calls=%fused_computation.20 | convolution fusion | flops 537001984 | bytes 4980736 | tf_op jit(solution)/shard_map/dot_general | solution.py:59
  89.4 0.4 copy.71
  89.8 0.5 broadcast.48
  90.3 2.2 %reduce = bf16[1024,128]{1,0:T(8,128)(2,1)S(1)} reduce(bf16[1024,1,128]{2,1,0:T(2,128)(2,1)S(1)} %bitcast.93, bf16[]{:T(256)} %broadcast.48), dimensions={1}, to_apply=%bitcast.66.reduce_sub_computation | reduce | bytes 524290
  92.5 0.8 reshape.70
  93.3 3.4 %all-to-all-start = ((bf16[4,2,16384]{2,1,0:T(2,128)(2,1)}), bf16[4,2,16384]{2,1,0:T(2,128)(2,1)S(1)}, u32[]{:S(2)}, u32[]{:S(2)}) async-start(bf16[4,2,16384]{2,1,0:T(2,128)(2,1)} %reshape.70), calls=%async_computation | async-start | bytes 524288 | tf_op jit(solution)/shard_map/all_to_all | solution.py:66
  96.7 3.4 %fusion.31 = (f32[4,512]{1,0:T(4,128)S(1)}, f32[4,512,512]{1,2,0:T(8,128)}) fusion(f32[4,512]{1,0:T(4,128)S(1)} %bitcast.114, pred[512,512]{0,1:T(8,128)(4,1)S(1)} %iota_compare_fusion, bf16[4,512,64]{1,2,0:T(8,128)(2,1)S(1)} %bitcast.99, bf16[4,512,64]{1,2,0:T(8,128)(2,1)S(1)} %bitcast.102), kind=kOutput, calls=%fused_computation.43 | convolution fusion | flops 140509696 | bytes 4997120 | tf_op jit(solution)/shard_map/while/body/eval_jaxpr/sub | solution.py:30
  100.1 56.5 %reduce-scatter.2.cloned.1.call-done = f32[128,512]{0,1:T(8,128)} async-done(((f32[1024,512]{0,1:T(8,128)}), f32[128,512]{0,1:T(8,128)}) %reduce-scatter.2.cloned.1.call-update) | async-done | bytes 262160 | tf_op jit(solution)/shard_map/reduce_scatter | solution.py:72
  156.6 1.8 copy.88
  158.4 0.0 all-to-all-done
  158.4 0.3 reshape.71
  158.8 0.2 copy.72
  159.0 0.1 reshape_squeeze.14
  159.1 0.0 copy-start.2
  159.1 0.1 multiply_reduce_fusion
  159.2 3.5 %fusion.30 = (f32[4,512]{1,0:T(4,128)S(1)}, f32[4,512]{1,0:T(4,128)S(1)}, bf16[4,512,512]{1,2,0:T(8,128)(2,1)S(1)}) fusion(f32[4,512]{1,0:T(4,128)S(1)} %multiply_reduce_fusion, bf16[4,512,64]{1,2,0:T(8,128)(2,1)} %bitcast.113, bf16[512,4,64]{0,2,1:T(8,128)(2,1)S(1)} %reshape_squeeze.14, f32[4,512,512]{1,2,0:T(8,128)} %get-tuple-element.76, ...), kind=kOutput, calls=%fused_computation.42 | convolution fusion | flops 140505088 | bytes 6848512 | tf_op jit(solution)/shard_map/while/body/eval_jaxpr/hqe,hke->hqk/dot_general | solution.py:15
  162.6 0.8 fusion.9
  163.4 0.4 copy.80
  163.8 0.0 copy-start.3
  163.8 3.0 %reduce.2 = bf16[512,256]{1,0:T(8,128)(2,1)} reduce(bf16[512,1,256]{2,1,0:T(2,128)(2,1)S(1)} %bitcast.95, bf16[]{:T(256)} %broadcast.48), dimensions={1}, to_apply=%bitcast.70.reduce_sub_computation | reduce | bytes 524290
  166.8 1.7 reshape.74
  168.5 3.6 %all-to-all-start.2 = ((bf16[4,2,16384]{2,1,0:T(2,128)(2,1)}), bf16[4,2,16384]{2,1,0:T(2,128)(2,1)S(1)}, u32[]{:S(2)}, u32[]{:S(2)}) async-start(bf16[4,2,16384]{2,1,0:T(2,128)(2,1)} %reshape.74), calls=%async_computation.2 | async-start | bytes 524288 | tf_op jit(solution)/shard_map/all_to_all | solution.py:107
  172.1 0.5 fusion.10
  172.6 0.4 copy.77
  173.0 2.2 %reduce.1 = bf16[512,256]{1,0:T(8,128)(2,1)S(1)} reduce(bf16[512,1,256]{2,1,0:T(2,128)(2,1)S(1)} %bitcast.96, bf16[]{:T(256)} %broadcast.48), dimensions={1}, to_apply=%bitcast.68.reduce_sub_computation | reduce | bytes 524290
  175.2 0.8 reshape.72
  176.0 1.9 all-to-all-done.2
  177.9 3.4 %all-to-all-start.1 = ((bf16[4,2,16384]{2,1,0:T(2,128)(2,1)}), bf16[4,2,16384]{2,1,0:T(2,128)(2,1)S(1)}, u32[]{:S(2)}, u32[]{:S(2)}) async-start(bf16[4,2,16384]{2,1,0:T(2,128)(2,1)} %reshape.72), calls=%async_computation.1 | async-start | bytes 524288 | tf_op jit(solution)/shard_map/all_to_all | solution.py:106
  181.3 0.0 copy-done.3
  181.3 3.2 %fusion.11 = bf16[4,512,64]{1,2,0:T(8,128)(2,1)S(1)} fusion(f32[4,512]{1,0:T(4,128)S(1)} %get-tuple-element.75, bf16[512,4,64]{0,2,1:T(8,128)(2,1)S(1)} %copy-done.3, f32[4,512]{1,0:T(4,128)S(1)} %bitcast.115, pred[512,512]{0,1:T(8,128)(4,1)} %copy-done.7, bf16[4,512,64]{1,2,0:T(8,128)(2,1)S(1)} %bitcast.101, bf16[4,512,64]{1,2,0:T(8,128)(2,1)S(1)} %bitcast.104), kind=kOutput, calls=%fused_computation.19 | convolution fusion | flops 275909120 | bytes 1327104 | tf_op jit(solution)/shard_map/while/body/eval_jaxpr/hqk,hqe->hke/dot_general | solution.py:15
  184.6 0.4 copy.83
  185.0 2.2 %reduce.3 = bf16[512,256]{1,0:T(8,128)(2,1)S(1)} reduce(bf16[512,1,256]{2,1,0:T(2,128)(2,1)S(1)} %bitcast.94, bf16[]{:T(256)} %broadcast.48), dimensions={1}, to_apply=%bitcast.72.reduce_sub_computation | reduce | bytes 524290
  187.2 0.8 reshape.76
  188.0 0.0 all-to-all-done.1
  188.0 3.4 %all-to-all-start.3 = ((bf16[4,2,16384]{2,1,0:T(2,128)(2,1)}), bf16[4,2,16384]{2,1,0:T(2,128)(2,1)S(1)}, u32[]{:S(2)}, u32[]{:S(2)}) async-start(bf16[4,2,16384]{2,1,0:T(2,128)(2,1)} %reshape.76), calls=%async_computation.3 | async-start | bytes 524288 | tf_op jit(solution)/shard_map/all_to_all | solution.py:108
  191.4 0.6 add_bitcast_fusion
  192.0 0.3 reshape.75
  192.3 0.2 copy.81
  192.5 0.9 copy.86
  193.3 0.3 reshape.73
  193.7 0.2 copy.78
  193.8 0.9 copy.85
  194.7 2.7 %all-to-all-done.3 = bf16[4,2,16384]{2,1,0:T(2,128)(2,1)S(1)} async-done(((bf16[4,2,16384]{2,1,0:T(2,128)(2,1)}), bf16[4,2,16384]{2,1,0:T(2,128)(2,1)S(1)}, u32[]{:S(2)}, u32[]{:S(2)}) %all-to-all-start.3) | async-done | bytes 262176 | tf_op jit(solution)/shard_map/all_to_all | solution.py:108
  197.4 0.3 reshape.77
  197.7 0.2 copy.84
  197.9 0.9 copy.87
  (16 shorter events, 0.2 us)
Async XLA Ops:
  7.2 15.0 %copy-start.1 = (bf16[1,512,1024]{2,1,0:T(8,128)(2,1)S(1)}, bf16[1,512,1024]{2,1,0:T(8,128)(2,1)}, u32[]{:S(2)}) copy-start(bf16[1,512,1024]{2,1,0:T(8,128)(2,1)} %param.10) | copy-start | bytes 3145732
  7.2 78.5 %all-gather.2.cloned.1.call-start = ((), (), s32[]{:S(2)}) async-start(), calls=%async_computation.6 | async-start | bytes 4718592 | tf_op jit(solution)/shard_map/all_gather | solution.py:61
  7.9 148.7 %reduce-scatter.2.cloned.1.call-start = ((), (), s32[]{:S(2)}) async-start(), calls=%async_computation.7 | async-start | bytes 2359296 | tf_op jit(solution)/shard_map/reduce_scatter | solution.py:72
  9.2 15.3 %copy-start.4 = (bf16[1,512,256]{2,1,0:T(8,128)(2,1)S(1)}, bf16[1,512,256]{2,1,0:T(8,128)(2,1)}, u32[]{:S(2)}) copy-start(bf16[1,512,256]{2,1,0:T(8,128)(2,1)} %param.7) | copy-start | bytes 786436
  22.2 2.5 %copy-start.5 = (bf16[1,512,256]{2,1,0:T(8,128)(2,1)S(1)}, bf16[1,512,256]{2,1,0:T(8,128)(2,1)}, u32[]{:S(2)}) copy-start(bf16[1,512,256]{2,1,0:T(8,128)(2,1)} %param.8) | copy-start | bytes 786436
  22.2 2.7 %copy-start.6 = (bf16[1,512,256]{2,1,0:T(8,128)(2,1)S(1)}, bf16[1,512,256]{2,1,0:T(8,128)(2,1)}, u32[]{:S(2)}) copy-start(bf16[1,512,256]{2,1,0:T(8,128)(2,1)} %param.9) | copy-start | bytes 786436
  22.2 63.5 %copy-start = (bf16[1,128,2048]{2,1,0:T(8,128)(2,1)S(1)}, bf16[1,128,2048]{2,1,0:T(8,128)(2,1)}, u32[]{:S(2)}) copy-start(bf16[1,128,2048]{2,1,0:T(8,128)(2,1)} %param.12) | copy-start | bytes 1572868
  24.8 71.9 %copy-start.8 = (f32[1,4,512]{2,1,0:T(4,128)S(1)}, f32[1,4,512]{2,1,0:T(4,128)}, u32[]{:S(2)}) copy-start(f32[1,4,512]{2,1,0:T(4,128)} %param.11) | copy-start | bytes 24580
  25.8 74.4 %copy-start.7 = (pred[512,512]{0,1:T(8,128)(4,1)}, pred[512,512]{0,1:T(8,128)(4,1)S(1)}, u32[]{:S(2)}) copy-start(pred[512,512]{0,1:T(8,128)(4,1)S(1)} %iota_compare_fusion) | copy-start | bytes 786436
  93.3 65.2 %all-to-all-start = ((bf16[4,2,16384]{2,1,0:T(2,128)(2,1)}), bf16[4,2,16384]{2,1,0:T(2,128)(2,1)S(1)}, u32[]{:S(2)}, u32[]{:S(2)}) async-start(bf16[4,2,16384]{2,1,0:T(2,128)(2,1)} %reshape.70), calls=%async_computation | async-start | bytes 524288 | tf_op jit(solution)/shard_map/all_to_all | solution.py:66
  159.1 3.6 %copy-start.2 = (bf16[512,4,64]{0,2,1:T(8,128)(2,1)}, bf16[512,4,64]{0,2,1:T(8,128)(2,1)S(1)}, u32[]{:S(2)}) copy-start(bf16[512,4,64]{0,2,1:T(8,128)(2,1)S(1)} %reshape_squeeze.14) | copy-start | bytes 786436
  163.8 17.5 %copy-start.3 = (bf16[512,4,64]{0,2,1:T(8,128)(2,1)S(1)}, bf16[512,4,64]{0,2,1:T(8,128)(2,1)}, u32[]{:S(2)}) copy-start(bf16[512,4,64]{0,2,1:T(8,128)(2,1)} %copy-done.2) | copy-start | bytes 786436
  168.5 9.4 %all-to-all-start.2 = ((bf16[4,2,16384]{2,1,0:T(2,128)(2,1)}), bf16[4,2,16384]{2,1,0:T(2,128)(2,1)S(1)}, u32[]{:S(2)}, u32[]{:S(2)}) async-start(bf16[4,2,16384]{2,1,0:T(2,128)(2,1)} %reshape.74), calls=%async_computation.2 | async-start | bytes 524288 | tf_op jit(solution)/shard_map/all_to_all | solution.py:107
  177.9 10.1 %all-to-all-start.1 = ((bf16[4,2,16384]{2,1,0:T(2,128)(2,1)}), bf16[4,2,16384]{2,1,0:T(2,128)(2,1)S(1)}, u32[]{:S(2)}, u32[]{:S(2)}) async-start(bf16[4,2,16384]{2,1,0:T(2,128)(2,1)} %reshape.72), calls=%async_computation.1 | async-start | bytes 524288 | tf_op jit(solution)/shard_map/all_to_all | solution.py:106
  188.0 9.4 %all-to-all-start.3 = ((bf16[4,2,16384]{2,1,0:T(2,128)(2,1)}), bf16[4,2,16384]{2,1,0:T(2,128)(2,1)S(1)}, u32[]{:S(2)}, u32[]{:S(2)}) async-start(bf16[4,2,16384]{2,1,0:T(2,128)(2,1)} %reshape.76), calls=%async_computation.3 | async-start | bytes 524288 | tf_op jit(solution)/shard_map/all_to_all | solution.py:108
Sparse Core Ops, SparseCore 0:
  10.1 75.5 all-gather.1
  89.2 67.3 reduce-scatter.1
